TPU v7x, 32 devices: a whole 2x2x4 slice. The times are simulated.
32 devices in a mesh: rep: 2 (over y), fs: 4 (over z), tp: 4 (over x, core).
Axes of the slice: x: 2, y: 2, z: 4, core: 2. Of those that a mesh axis runs over, the one named last changes fastest.
Arguments:
- stream: bfloat16 [4096, 2048], P(('rep', 'fs', 'tp')), may hold values from -6 to 6
- gain_before: float32 [2048], replicated, may hold values from 0.1 to 1.9
- gain_after: float32 [2048], replicated, may hold values from 0.1 to 1.9
- proj_gate: bfloat16 [2048, 3584], P('fs', 'tp'), may hold values from -0.125 to 0.125
- proj_lift: bfloat16 [2048, 3584], P('fs', 'tp'), may hold values from -0.125 to 0.125
- proj_down: bfloat16 [3584, 2048], P('tp', 'fs'), may hold values from -0.09375 to 0.09375
- mixer_gain: float32 [2048], replicated, may hold values from 0.1 to 1.9
- mixer_u: bfloat16 [2048, 2048], P('fs', 'tp'), may hold values from -0.125 to 0.125
- mixer_v: bfloat16 [2048, 2048], P('fs', 'tp'), may hold values from -1 to 1
- layer_gain: float32 [2048], P('tp'), may hold values from 0.1 to 1.9
- layer_shift: float32 [2048], P('tp'), may hold values from -3 to 3
- spatial: bfloat16 [16, 128, 128], P('tp'), may hold values from -0.5 to 0.5
- spatial_shift: float32 [16, 128], P('tp'), may hold values from 0.2 to 2
- mixer_down: bfloat16 [2048, 2048], P('tp', 'fs'), may hold values from -0.125 to 0.125
Outputs:
- result: bfloat16 [4096, 2048], P(('rep', 'fs', 'tp'))
All inputs are finite; a program needn't handle non-finite values.
Results may differ from a plain program's by a relative error of at most 0.017.
Values may be sent and summed in bfloat16 or wider, within the bound.
A program may use at most 128 MiB of HBM per device.

v0:
```python
import jax
import jax.numpy as jnp
from jax import lax
from jax.sharding import PartitionSpec as P

GROUP_DIM = 128
SPAN = 128
A = 2048
norm_epsilon = 1e-06
layer_epsilon = 1e-05


def norm_rows(row_block, scale_gain):
    widened = row_block.astype(jnp.float32)
    factor = lax.rsqrt(jnp.mean(widened * widened, axis=1, keepdims=True) + norm_epsilon)
    return (widened * factor * scale_gain).astype(jnp.bfloat16)


def gathered_norm(stream_rows, scale_gain):
    gathered = lax.all_gather(stream_rows, "tp", axis=0, tiled=True)
    return norm_rows(gathered, scale_gain)


def pair_adder(normed, pieces):
    return (
        jnp.dot(normed, pieces[0], preferred_element_type=jnp.float32),
        jnp.dot(normed, pieces[1], preferred_element_type=jnp.float32),
    )


def activate(gate_vals, lift_vals):
    return (jax.nn.silu(gate_vals) * lift_vals).astype(jnp.bfloat16)


def half_again(stream_rows, scale_gain, proj_gate, proj_lift, proj_down):
    normed = gathered_norm(stream_rows, scale_gain)
    gate_vals, lift_vals = pair_adder(
        normed,
        (
            lax.all_gather(proj_gate, "fs", axis=0, tiled=True),
            lax.all_gather(proj_lift, "fs", axis=0, tiled=True),
        ),
    )
    hidden = activate(gate_vals, lift_vals)
    partial_value = jnp.dot(
        hidden,
        lax.all_gather(proj_down, "fs", axis=1, tiled=True),
        preferred_element_type=jnp.float32,
    )
    summed = lax.psum_scatter(
        partial_value.astype(jnp.bfloat16), "tp", scatter_dimension=0, tiled=True
    ).astype(jnp.float32)
    return (stream_rows.astype(jnp.float32) + 0.5 * summed).astype(jnp.bfloat16)


def token_mixer(
    stream_rows,
    mixer_gain,
    mixer_u,
    mixer_v,
    layer_gain,
    layer_shift,
    spatial,
    spatial_shift,
    mixer_down,
):
    gathered = lax.all_gather(stream_rows, "tp", axis=0, tiled=True)
    normed = norm_rows(gathered, mixer_gain)
    seq_tokens = normed.shape[0]
    u_vals, v_vals = pair_adder(
        normed,
        (
            lax.all_gather(mixer_u, "fs", axis=0, tiled=True),
            lax.all_gather(mixer_v, "fs", axis=0, tiled=True),
        ),
    )
    lifted = jax.nn.gelu(v_vals)
    moments = lax.psum((jnp.sum(lifted, axis=1), jnp.sum(lifted * lifted, axis=1)), "tp")
    centre = moments[0] / A
    spread = moments[1] / A - centre * centre
    normed_v = (
        (lifted - centre[:, None]) * lax.rsqrt(spread[:, None] + layer_epsilon) * layer_gain
        + layer_shift
    ).astype(jnp.bfloat16)
    groups_here = spatial.shape[0]
    blocked = normed_v.reshape(seq_tokens // SPAN, SPAN, groups_here, GROUP_DIM)
    causal = jnp.tril(jnp.ones((SPAN, SPAN), dtype=bool))
    masked = jnp.where(causal[None], spatial, jnp.zeros((), jnp.bfloat16))
    mixed_v = jnp.einsum("gts,bsgd->btgd", masked, blocked, preferred_element_type=jnp.float32)
    mixed_v = mixed_v + spatial_shift.T[None, :, :, None]
    gated = (jax.nn.gelu(u_vals) * mixed_v.reshape(seq_tokens, groups_here * GROUP_DIM)).astype(
        jnp.bfloat16
    )
    partial_value = jnp.dot(
        gated,
        lax.all_gather(mixer_down, "fs", axis=1, tiled=True),
        preferred_element_type=jnp.float32,
    )
    summed = lax.psum_scatter(
        partial_value.astype(jnp.bfloat16), "tp", scatter_dimension=0, tiled=True
    ).astype(jnp.float32)
    return (stream_rows.astype(jnp.float32) + summed).astype(jnp.bfloat16)


def body(
    stream,
    gain_before,
    gain_after,
    proj_gate,
    proj_lift,
    proj_down,
    mixer_gain,
    mixer_u,
    mixer_v,
    layer_gain,
    layer_shift,
    spatial,
    spatial_shift,
    mixer_down,
):
    first = half_again(stream, gain_before, proj_gate, proj_lift, proj_down)
    second = token_mixer(
        first,
        mixer_gain,
        mixer_u,
        mixer_v,
        layer_gain,
        layer_shift,
        spatial,
        spatial_shift,
        mixer_down,
    )
    result = half_again(second, gain_after, proj_gate, proj_lift, proj_down)
    return result


def solution(mesh):
    placed = (
        P(("rep", "fs", "tp"), None),
        P(),
        P(),
        P("fs", "tp"),
        P("fs", "tp"),
        P("tp", "fs"),
        P(),
        P("fs", "tp"),
        P("fs", "tp"),
        P("tp"),
        P("tp"),
        P("tp", None, None),
        P("tp", None),
        P("tp", "fs"),
    )
    return jax.shard_map(
        body, mesh=mesh, in_specs=placed, out_specs=P(("rep", "fs", "tp"), None), check_vma=False
    )
```

profile of v0, /device:TPU:0, one launch (start us, length us, event | category | flops | bytes accessed | tf_op | source)
XLA Modules:
  0.0 575.2 jit_solution(15976335767558670113)
XLA Ops:
  6.5 0.7 all-gather.10.cloned.1.call-update
  7.3 0.7 all-gather.12.cloned.1.call-update
  9.4 24.8 %all-gather.10.cloned.1.call-done = bf16[512,2048]{1,0:T(8,128)(2,1)} async-done(((bf16[128,2048]{1,0:T(8,128)(2,1)}), bf16[512,2048]{1,0:T(8,128)(2,1)}) %all-gather.10.cloned.1.call-update) | async-done | bytes 2097168 | tf_op jit(solution)/shard_map/all_gather | solution.py:20
  34.2 2.2 fusion
  36.4 71.5 %all-gather.12.cloned.1.call-done = bf16[2048,896]{1,0:T(8,128)(2,1)} async-done(((bf16[512,896]{1,0:T(8,128)(2,1)}), bf16[2048,896]{1,0:T(8,128)(2,1)}) %all-gather.12.cloned.1.call-update) | async-done | bytes 3670032 | tf_op jit(solution)/shard_map/all_gather | solution.py:40
  107.9 5.6 fusion.42
  113.5 66.6 %all-gather.14.cloned.1.call-done = bf16[2048,896]{1,0:T(8,128)(2,1)} async-done(((bf16[512,896]{1,0:T(8,128)(2,1)}), bf16[2048,896]{1,0:T(8,128)(2,1)}) %all-gather.14.cloned.1.call-update) | async-done | bytes 3670032 | tf_op jit(solution)/shard_map/all_gather | solution.py:41
  180.2 72.1 %all-gather.16.cloned.1.call-done = bf16[896,2048]{1,0:T(8,128)(2,1)} async-done(((bf16[896,512]{1,0:T(8,128)(2,1)}), bf16[896,2048]{1,0:T(8,128)(2,1)}) %all-gather.16.cloned.1.call-update) | async-done | bytes 3670032 | tf_op jit(solution)/shard_map/all_gather | solution.py:47
  252.3 9.7 %convolution_convert_fusion.1 = bf16[512,2048]{1,0:T(8,128)(2,1)} fusion(bf16[896,2048]{1,0:T(8,128)(2,1)} %all-gather.16.cloned.1.call-done, f32[512,896]{1,0:T(8,128)} %fusion.42, bf16[2048,896]{1,0:T(8,128)(2,1)} %all-gather.14.cloned.1.call-done, bf16[512,2048]{1,0:T(8,128)(2,1)S(1)} %copy-done.4, f32[2048]{0:T(1024)S(1)} %copy-done.10, ...), kind=kOutput, calls=%fused_computation.16 | convolution fusion | flops 3766091776 | bytes 13379584 | tf_op jit(solution)/shard_map/dot_general | solution.py:45
  262.0 29.9 %reduce-scatter.4.cloned.1.call-done = bf16[128,2048]{1,0:T(8,128)(2,1)} async-done(((bf16[512,2048]{1,0:T(8,128)(2,1)}), bf16[128,2048]{1,0:T(8,128)(2,1)}) %reduce-scatter.4.cloned.1.call-update) | async-done | bytes 524304 | tf_op jit(solution)/shard_map/reduce_scatter | solution.py:50
  291.9 2.0 add_convert_fusion.3
  294.0 0.7 all-gather.22.cloned.1.call-update
  296.2 20.4 %all-gather.18.cloned.1.call-done = bf16[512,2048]{1,0:T(8,128)(2,1)} async-done(((bf16[128,2048]{1,0:T(8,128)(2,1)}), bf16[512,2048]{1,0:T(8,128)(2,1)}) %all-gather.18.cloned.1.call-update) | async-done | bytes 2097168 | tf_op jit(solution)/shard_map/all_gather | solution.py:67
  316.6 2.2 fusion.3
  318.9 45.0 %all-gather.22.cloned.1.call-done = bf16[2048,512]{1,0:T(8,128)(2,1)} async-done(((bf16[512,512]{1,0:T(8,128)(2,1)}), bf16[2048,512]{1,0:T(8,128)(2,1)}) %all-gather.22.cloned.1.call-update) | async-done | bytes 2097168 | tf_op jit(solution)/shard_map/all_gather | solution.py:74
  363.9 4.1 fusion.60
  368.0 6.5 %all-reduce = (f32[512]{0:T(512)S(1)}, f32[512]{0:T(512)S(1)}) all-reduce(f32[512]{0:T(512)S(1)} %get-tuple-element.6, f32[512]{0:T(512)S(1)} %get-tuple-element.5), channel_id=1, replica_groups=mesh['rep'=2,'fs'=4,'tp'=4] {'tp'}, use_global_device_ids=true, to_apply=%region_6.7 | all-reduce | flops 1024 | bytes 8192 | tf_op jit(solution)/shard_map/psum | solution.py:78
  374.6 1.5 add_convert_fusion.2
  376.0 0.9 reshape.47
  377.0 1.4 fusion.9
  378.4 1.3 copy.21
  379.7 30.2 %all-gather.20.cloned.1.call-done = bf16[2048,512]{1,0:T(8,128)(2,1)} async-done(((bf16[512,512]{1,0:T(8,128)(2,1)}), bf16[2048,512]{1,0:T(8,128)(2,1)}) %all-gather.20.cloned.1.call-update) | async-done | bytes 2097168 | tf_op jit(solution)/shard_map/all_gather | solution.py:73
  409.9 46.1 %all-gather.24.cloned.1.call-done = bf16[512,2048]{1,0:T(8,128)(2,1)} async-done(((bf16[512,512]{1,0:T(8,128)(2,1)}), bf16[512,2048]{1,0:T(8,128)(2,1)}) %all-gather.24.cloned.1.call-update) | async-done | bytes 2097168 | tf_op jit(solution)/shard_map/all_gather | solution.py:96
  456.0 6.5 %convolution_convert_fusion.2 = bf16[512,2048]{1,0:T(8,128)(2,1)} fusion(bf16[512,2048]{1,0:T(8,128)(2,1)} %all-gather.24.cloned.1.call-done, f32[64,8,4,128]{3,2,1,0:T(4,128)} %bitcast.25, bf16[2048,512]{1,0:T(8,128)(2,1)} %all-gather.20.cloned.1.call-done, bf16[512,2048]{1,0:T(8,128)(2,1)S(1)} %copy-done.3, f32[2048]{0:T(1024)S(1)} %copy-done.11, ...), kind=kOutput, calls=%fused_computation.17 | convolution fusion | flops 2155347968 | bytes 9447424 | tf_op jit(solution)/shard_map/dot_general | solution.py:94
  462.6 30.1 %reduce-scatter.6.cloned.1.call-done = bf16[128,2048]{1,0:T(8,128)(2,1)} async-done(((bf16[512,2048]{1,0:T(8,128)(2,1)}), bf16[128,2048]{1,0:T(8,128)(2,1)}) %reduce-scatter.6.cloned.1.call-update) | async-done | bytes 524304 | tf_op jit(solution)/shard_map/reduce_scatter | solution.py:99
  492.7 2.0 add_convert_fusion.1
  494.9 22.5 %all-gather.26.cloned.1.call-done = bf16[512,2048]{1,0:T(8,128)(2,1)} async-done(((bf16[128,2048]{1,0:T(8,128)(2,1)}), bf16[512,2048]{1,0:T(8,128)(2,1)}) %all-gather.26.cloned.1.call-update) | async-done | bytes 2097168 | tf_op jit(solution)/shard_map/all_gather | solution.py:20
  517.4 2.2 fusion.6
  519.6 5.7 fusion.28
  525.3 9.7 %convolution_convert_fusion = bf16[512,2048]{1,0:T(8,128)(2,1)} fusion(bf16[896,2048]{1,0:T(8,128)(2,1)} %all-gather.16.cloned.1.call-done, f32[512,896]{1,0:T(8,128)} %fusion.28, bf16[2048,896]{1,0:T(8,128)(2,1)} %all-gather.14.cloned.1.call-done, bf16[512,2048]{1,0:T(8,128)(2,1)S(1)} %copy-done.5, f32[2048]{0:T(1024)S(1)} %copy-done.12, ...), kind=kOutput, calls=%fused_computation.15 | convolution fusion | flops 3766091776 | bytes 13379584 | tf_op jit(solution)/shard_map/dot_general | solution.py:45
  535.0 31.3 %reduce-scatter.8.cloned.1.call-done = bf16[128,2048]{1,0:T(8,128)(2,1)} async-done(((bf16[512,2048]{1,0:T(8,128)(2,1)}), bf16[128,2048]{1,0:T(8,128)(2,1)}) %reduce-scatter.8.cloned.1.call-update) | async-done | bytes 524304 | tf_op jit(solution)/shard_map/reduce_scatter | solution.py:50
  566.4 2.0 add_convert_fusion
  (52 shorter events, 3.4 us)
Async XLA Ops:
  6.5 27.7 %all-gather.10.cloned.1.call-start = ((), (), s32[]{:S(2)}) async-start(), calls=%async_computation.3 | async-start | bytes 2621440 | tf_op jit(solution)/shard_map/all_gather | solution.py:20
  7.3 100.6 %all-gather.12.cloned.1.call-start = ((), (), s32[]{:S(2)}) async-start(), calls=%async_computation.4 | async-start | bytes 4587520 | tf_op jit(solution)/shard_map/all_gather | solution.py:40
  8.0 99.9 %copy-start.10 = (f32[2048]{0:T(1024)S(1)}, f32[2048]{0:T(1024)}, u32[]{:S(2)}) copy-start(f32[2048]{0:T(1024)} %param.15) | copy-start | bytes 24580
  8.0 172.2 %all-gather.14.cloned.1.call-start = ((), (), s32[]{:S(2)}) async-start(), calls=%async_computation.5 | async-start | bytes 4587520 | tf_op jit(solution)/shard_map/all_gather | solution.py:41
  8.8 243.5 %all-gather.16.cloned.1.call-start = ((), (), s32[]{:S(2)}) async-start(), calls=%async_computation.6 | async-start | bytes 4587520 | tf_op jit(solution)/shard_map/all_gather | solution.py:47
  9.3 282.6 %reduce-scatter.4.cloned.1.call-start = ((), (), s32[]{:S(2)}) async-start(), calls=%async_computation.7 | async-start | bytes 2621440 | tf_op jit(solution)/shard_map/reduce_scatter | solution.py:50
  34.2 73.7 %copy-start.4 = (bf16[512,2048]{1,0:T(8,128)(2,1)S(1)}, bf16[512,2048]{1,0:T(8,128)(2,1)}, u32[]{:S(2)}) copy-start(bf16[512,2048]{1,0:T(8,128)(2,1)} %all-gather.10.cloned.1.call-done) | copy-start | bytes 6291460
  262.0 29.9 %copy-start.2 = (bf16[128,2048]{1,0:T(8,128)(2,1)S(1)}, bf16[128,2048]{1,0:T(8,128)(2,1)}, u32[]{:S(2)}) copy-start(bf16[128,2048]{1,0:T(8,128)(2,1)} %param.14) | copy-start | bytes 1572868
  262.0 54.6 %all-gather.18.cloned.1.call-start = ((), (), s32[]{:S(2)}) async-start(), calls=%async_computation.8 | async-start | bytes 2621440 | tf_op jit(solution)/shard_map/all_gather | solution.py:67
  293.9 70.0 %copy-start.11 = (f32[2048]{0:T(1024)S(1)}, f32[2048]{0:T(1024)}, u32[]{:S(2)}) copy-start(f32[2048]{0:T(1024)} %param.20) | copy-start | bytes 24580
  293.9 70.0 %all-gather.22.cloned.1.call-start = ((), (), s32[]{:S(2)}) async-start(), calls=%async_computation.10 | async-start | bytes 2621440 | tf_op jit(solution)/shard_map/all_gather | solution.py:74
  294.7 115.3 %all-gather.20.cloned.1.call-start = ((), (), s32[]{:S(2)}) async-start(), calls=%async_computation.9 | async-start | bytes 2621440 | tf_op jit(solution)/shard_map/all_gather | solution.py:73
  295.4 160.6 %all-gather.24.cloned.1.call-start = ((), (), s32[]{:S(2)}) async-start(), calls=%async_computation.11 | async-start | bytes 2621440 | tf_op jit(solution)/shard_map/all_gather | solution.py:96
  296.2 196.5 %reduce-scatter.6.cloned.1.call-start = ((), (), s32[]{:S(2)}) async-start(), calls=%async_computation.12 | async-start | bytes 2621440 | tf_op jit(solution)/shard_map/reduce_scatter | solution.py:99
  316.6 47.3 %copy-start.3 = (bf16[512,2048]{1,0:T(8,128)(2,1)S(1)}, bf16[512,2048]{1,0:T(8,128)(2,1)}, u32[]{:S(2)}) copy-start(bf16[512,2048]{1,0:T(8,128)(2,1)} %all-gather.18.cloned.1.call-done) | copy-start | bytes 6291460
  318.9 55.7 %copy-start.7 = (f32[512]{0:T(512)S(1)}, f32[512]{0:T(512)}, u32[]{:S(2)}) copy-start(f32[512]{0:T(512)} %param.24) | copy-start | bytes 6148
  318.9 55.7 %copy-start.8 = (f32[512]{0:T(512)S(1)}, f32[512]{0:T(512)}, u32[]{:S(2)}) copy-start(f32[512]{0:T(512)} %param.23) | copy-start | bytes 6148
  368.0 8.9 %copy-start.6 = (bf16[4,128,128]{2,1,0:T(8,128)(2,1)S(1)}, bf16[4,128,128]{2,1,0:T(8,128)(2,1)}, u32[]{:S(2)}) copy-start(bf16[4,128,128]{2,1,0:T(8,128)(2,1)} %param.25) | copy-start | bytes 393220
  368.0 8.9 %copy-start.9 = (f32[4,128]{1,0:T(4,128)S(1)}, f32[4,128]{1,0:T(4,128)}, u32[]{:S(2)}) copy-start(f32[4,128]{1,0:T(4,128)} %param.26) | copy-start | bytes 6148
  462.5 30.2 %copy-start = (bf16[128,2048]{1,0:T(8,128)(2,1)S(1)}, bf16[128,2048]{1,0:T(8,128)(2,1)}, u32[]{:S(2)}) copy-start(bf16[128,2048]{1,0:T(8,128)(2,1)} %add_convert_fusion.3) | copy-start | bytes 1572868
  462.5 57.1 %copy-start.12 = (f32[2048]{0:T(1024)S(1)}, f32[2048]{0:T(1024)}, u32[]{:S(2)}) copy-start(f32[2048]{0:T(1024)} %param.16) | copy-start | bytes 24580
  462.5 54.8 %all-gather.26.cloned.1.call-start = ((), (), s32[]{:S(2)}) async-start(), calls=%async_computation.13 | async-start | bytes 2621440 | tf_op jit(solution)/shard_map/all_gather | solution.py:20
  494.6 71.7 %reduce-scatter.8.cloned.1.call-start = ((), (), s32[]{:S(2)}) async-start(), calls=%async_computation.14 | async-start | bytes 2621440 | tf_op jit(solution)/shard_map/reduce_scatter | solution.py:50
  517.4 2.2 copy-start.5
  535.0 31.4 %copy-start.1 = (bf16[128,2048]{1,0:T(8,128)(2,1)S(1)}, bf16[128,2048]{1,0:T(8,128)(2,1)}, u32[]{:S(2)}) copy-start(bf16[128,2048]{1,0:T(8,128)(2,1)} %add_convert_fusion.1) | copy-start | bytes 1572868
Sparse Core Ops, SparseCore 0:
  8.9 25.2 all-gather.9
  35.8 72.0 all-gather.11
  109.5 70.6 all-gather.13
  181.6 70.6 all-gather.15
  262.1 29.7 reduce-scatter.3
  294.1 22.5 all-gather.17
  318.2 45.6 all-gather.21
  365.5 44.4 all-gather.19
  411.5 44.4 all-gather.23
  462.6 29.9 reduce-scatter.5
  494.8 22.5 all-gather.25
  535.1 31.1 reduce-scatter.7
where the time goes:
time: 576 us; the launch traced here: 575 us
  waiting for transfers between devices  495 us (86%)
  matrix products  42.7 us (7%)
  other arithmetic  14.1 us (2%)
  between operations  13.7 us (2%)
  blocking collectives  6.51 us (1%)
    all_gather x1, waiting for transfers between devices, half_again(): lax.all_gather(proj_down, 'fs', axis=1, tiled=True)  72.1 us
    all_gather x1, waiting for transfers between devices, half_again(): lax.all_gather(proj_gate, 'fs', axis=0, tiled=True)  71.5 us
    all_gather x1, waiting for transfers between devices, half_again(): lax.all_gather(proj_lift, 'fs', axis=0, tiled=True)  66.6 us
    reduce_scatter x2, waiting for transfers between devices, half_again(): lax.psum_scatter(partial_value.astype(jnp.bfloat16), 'tp', scatter_dimens...  61.2 us
    all_gather x2, waiting for transfers between devices, gathered_norm(): gathered = lax.all_gather(stream_rows, 'tp', axis=0, tiled=True)  47.3 us
    all_gather x1, waiting for transfers between devices, token_mixer(): lax.all_gather(mixer_down, 'fs', axis=1, tiled=True)  46.1 us
    all_gather x1, waiting for transfers between devices, token_mixer(): lax.all_gather(mixer_v, 'fs', axis=0, tiled=True)  45 us
    all_gather x1, waiting for transfers between devices, token_mixer(): lax.all_gather(mixer_u, 'fs', axis=0, tiled=True)  30.2 us
  transfers between devices with their start and end apart: 12, of which 12 were waited for; matrix products, arithmetic and copies ran while one was open for 3% of the time, Pallas kernels for 0%

commit v1 on v0

--- a/solution.py
+++ b/solution.py
@@ -17,7 +17,12 @@
 
 
 def gathered_norm(stream_rows, scale_gain):
-    gathered = lax.all_gather(stream_rows, "tp", axis=0, tiled=True)
+    ring = [stream_rows]
+    for hop in range(3):
+        ring.append(lax.ppermute(ring[-1], "tp", [(dev, (dev + 1) % 4) for dev in range(4)]))
+    gathered = jnp.roll(
+        jnp.concatenate(ring[::-1], axis=0), (lax.axis_index("tp") + 1) * ring[0].shape[0], axis=0
+    )
     return norm_rows(gathered, scale_gain)
 
 

time: 576 us -> 553 us (0.960)
  waiting for transfers between devices: 495 us -> 471 us
    ppermute x0 -> x6, waiting for transfers between devices: none -> 52.1 us  [gathered_norm(): lax.ppermute(ring[-1], 'tp', [(dev, (dev + 1) % 4) for dev in range(4)])]
    all_gather x2 -> x0, waiting for transfers between devices: 47.3 us -> none  [gathered_norm(): gathered = lax.all_gather(stream_rows, 'tp', axis=0, tiled=True)]
    all_gather x1, waiting for transfers between devices: 71.5 us -> 43.7 us  [half_again(): lax.all_gather(proj_gate, 'fs', axis=0, tiled=True)]
  transfers between devices with their start and end apart: 12 -> 16, of which waited for: 12 -> 16; matrix products, arithmetic and copies ran while one was open for 3% -> 4% of each run, Pallas kernels for 0% -> 0%
where the time goes in v1:
time: 553 us
  waiting for transfers between devices  471 us (85%)
  matrix products  41.4 us (7%)
  other arithmetic  16.9 us (3%)
  between operations  13.7 us (2%)
  blocking collectives  6.68 us (1%)
    all_gather x1, waiting for transfers between devices, half_again(): lax.all_gather(proj_down, 'fs', axis=1, tiled=True)  72.3 us
    all_gather x1, waiting for transfers between devices, half_again(): lax.all_gather(proj_lift, 'fs', axis=0, tiled=True)  66.6 us
    reduce_scatter x2, waiting for transfers between devices, half_again(): lax.psum_scatter(partial_value.astype(jnp.bfloat16), 'tp', scatter_dimens...  61.1 us
    ppermute x6, waiting for transfers between devices, gathered_norm(): lax.ppermute(ring[-1], 'tp', [(dev, (dev + 1) % 4) for dev in range(4)])  52.1 us
    all_gather x1, waiting for transfers between devices, token_mixer(): lax.all_gather(mixer_down, 'fs', axis=1, tiled=True)  46.1 us
    all_gather x1, waiting for transfers between devices, token_mixer(): lax.all_gather(mixer_v, 'fs', axis=0, tiled=True)  45 us
    all_gather x1, waiting for transfers between devices, half_again(): lax.all_gather(proj_gate, 'fs', axis=0, tiled=True)  43.7 us
    reduce_scatter x1, waiting for transfers between devices, token_mixer(): lax.psum_scatter(partial_value.astype(jnp.bfloat16), 'tp', scatter_dimens...  30.1 us
  transfers between devices with their start and end apart: 16, of which 16 were waited for; matrix products, arithmetic and copies ran while one was open for 4% of the time, Pallas kernels for 0%

profile of v1, /device:TPU:0, one launch (start us, length us, event | category | flops | bytes accessed | tf_op | source)
XLA Modules:
  0.0 553.0 jit_solution(13497951438309852413)
XLA Ops:
  9.3 9.0 %collective-permute-done = bf16[128,2048]{1,0:T(8,128)(2,1)S(1)} collective-permute-done((bf16[128,2048]{1,0:T(8,128)(2,1)}, bf16[128,2048]{1,0:T(8,128)(2,1)S(1)}, u32[]{:S(2)}, u32[]{:S(2)}) %collective-permute-start) | collective-permute-done | bytes 524320 | tf_op jit(solution)/shard_map/ppermute | solution.py:22
  18.4 8.6 %collective-permute-done.1 = bf16[128,2048]{1,0:T(8,128)(2,1)S(1)} collective-permute-done((bf16[128,2048]{1,0:T(8,128)(2,1)S(1)}, bf16[128,2048]{1,0:T(8,128)(2,1)S(1)}, u32[]{:S(2)}, u32[]{:S(2)}) %collective-permute-start.1) | collective-permute-done | bytes 524320 | tf_op jit(solution)/shard_map/ppermute | solution.py:22
  26.9 8.7 %collective-permute-done.2 = bf16[128,2048]{1,0:T(8,128)(2,1)} collective-permute-done((bf16[128,2048]{1,0:T(8,128)(2,1)S(1)}, bf16[128,2048]{1,0:T(8,128)(2,1)}, u32[]{:S(2)}, u32[]{:S(2)}) %collective-permute-start.2) | collective-permute-done | bytes 524320 | tf_op jit(solution)/shard_map/ppermute | solution.py:22
  35.6 4.4 fusion
  40.1 43.7 %all-gather.8.cloned.1.call-done = bf16[2048,896]{1,0:T(8,128)(2,1)} async-done(((bf16[512,896]{1,0:T(8,128)(2,1)}), bf16[2048,896]{1,0:T(8,128)(2,1)}) %all-gather.8.cloned.1.call-update) | async-done | bytes 3670032 | tf_op jit(solution)/shard_map/all_gather | solution.py:45
  83.8 5.6 %fusion.56 = f32[512,896]{1,0:T(8,128)} fusion(bf16[2048,896]{1,0:T(8,128)(2,1)} %all-gather.8.cloned.1.call-done, bf16[512,2048]{1,0:T(8,128)(2,1)S(1)} %get-tuple-element.13, f32[2048]{0:T(1024)S(1)} %copy-done.8, f32[512]{0:T(512)S(1)} %add_rsqrt_fusion.3), kind=kOutput, calls=%fused_computation.78 | convolution fusion | flops 1883242496 | bytes 7612416 | tf_op jit(solution)/shard_map/dot_general | solution.py:31
  89.4 66.6 %all-gather.10.cloned.1.call-done = bf16[2048,896]{1,0:T(8,128)(2,1)} async-done(((bf16[512,896]{1,0:T(8,128)(2,1)}), bf16[2048,896]{1,0:T(8,128)(2,1)}) %all-gather.10.cloned.1.call-update) | async-done | bytes 3670032 | tf_op jit(solution)/shard_map/all_gather | solution.py:46
  156.0 72.3 %all-gather.12.cloned.1.call-done = bf16[896,2048]{1,0:T(8,128)(2,1)} async-done(((bf16[896,512]{1,0:T(8,128)(2,1)}), bf16[896,2048]{1,0:T(8,128)(2,1)}) %all-gather.12.cloned.1.call-update) | async-done | bytes 3670032 | tf_op jit(solution)/shard_map/all_gather | solution.py:52
  228.3 9.7 %convolution_convert_fusion.1 = bf16[512,2048]{1,0:T(8,128)(2,1)} fusion(bf16[896,2048]{1,0:T(8,128)(2,1)} %all-gather.12.cloned.1.call-done, f32[512,896]{1,0:T(8,128)} %fusion.56, bf16[2048,896]{1,0:T(8,128)(2,1)} %all-gather.10.cloned.1.call-done, bf16[512,2048]{1,0:T(8,128)(2,1)S(1)} %get-tuple-element.13, f32[2048]{0:T(1024)S(1)} %copy-done.8, ...), kind=kOutput, calls=%fused_computation.32 | convolution fusion | flops 3766091776 | bytes 13379584 | tf_op jit(solution)/shard_map/dot_general | solution.py:50
  238.0 29.8 %reduce-scatter.4.cloned.1.call-done = bf16[128,2048]{1,0:T(8,128)(2,1)} async-done(((bf16[512,2048]{1,0:T(8,128)(2,1)}), bf16[128,2048]{1,0:T(8,128)(2,1)}) %reduce-scatter.4.cloned.1.call-update) | async-done | bytes 524304 | tf_op jit(solution)/shard_map/reduce_scatter | solution.py:55
  267.9 2.0 add_convert_fusion.3
  272.0 20.6 %all-gather.14.cloned.1.call-done = bf16[512,2048]{1,0:T(8,128)(2,1)} async-done(((bf16[128,2048]{1,0:T(8,128)(2,1)}), bf16[512,2048]{1,0:T(8,128)(2,1)}) %all-gather.14.cloned.1.call-update) | async-done | bytes 2097168 | tf_op jit(solution)/shard_map/all_gather | solution.py:72
  292.6 2.1 fusion.3
  294.7 45.0 %all-gather.18.cloned.1.call-done = bf16[2048,512]{1,0:T(8,128)(2,1)} async-done(((bf16[512,512]{1,0:T(8,128)(2,1)}), bf16[2048,512]{1,0:T(8,128)(2,1)}) %all-gather.18.cloned.1.call-update) | async-done | bytes 2097168 | tf_op jit(solution)/shard_map/all_gather | solution.py:79
  339.7 4.7 fusion.74
  344.5 6.7 %all-reduce = (f32[512]{0:T(512)S(1)}, f32[512]{0:T(512)S(1)}) all-reduce(f32[512]{0:T(512)S(1)} %get-tuple-element.7, f32[512]{0:T(512)S(1)} %get-tuple-element.6), channel_id=1, replica_groups=mesh['rep'=2,'fs'=4,'tp'=4] {'tp'}, use_global_device_ids=true, to_apply=%region_6.8 | all-reduce | flops 1024 | bytes 8192 | tf_op jit(solution)/shard_map/psum | solution.py:83
  351.2 1.5 add_convert_fusion.2
  353.6 1.4 fusion.23
  355.0 1.3 copy.21
  356.3 29.5 %all-gather.16.cloned.1.call-done = bf16[2048,512]{1,0:T(8,128)(2,1)} async-done(((bf16[512,512]{1,0:T(8,128)(2,1)}), bf16[2048,512]{1,0:T(8,128)(2,1)}) %all-gather.16.cloned.1.call-update) | async-done | bytes 2097168 | tf_op jit(solution)/shard_map/all_gather | solution.py:78
  385.8 46.1 %all-gather.20.cloned.1.call-done = bf16[512,2048]{1,0:T(8,128)(2,1)} async-done(((bf16[512,512]{1,0:T(8,128)(2,1)}), bf16[512,2048]{1,0:T(8,128)(2,1)}) %all-gather.20.cloned.1.call-update) | async-done | bytes 2097168 | tf_op jit(solution)/shard_map/all_gather | solution.py:101
  431.9 6.6 %convolution_convert_fusion.2 = bf16[512,2048]{1,0:T(8,128)(2,1)} fusion(bf16[512,2048]{1,0:T(8,128)(2,1)} %all-gather.20.cloned.1.call-done, f32[64,8,4,128]{3,2,1,0:T(4,128)} %bitcast.25, bf16[2048,512]{1,0:T(8,128)(2,1)} %all-gather.16.cloned.1.call-done, bf16[512,2048]{1,0:T(8,128)(2,1)S(1)} %copy-done.1, f32[2048]{0:T(1024)S(1)} %copy-done.9, ...), kind=kOutput, calls=%fused_computation.33 | convolution fusion | flops 2155347968 | bytes 9447424 | tf_op jit(solution)/shard_map/dot_general | solution.py:99
  438.6 30.1 %reduce-scatter.6.cloned.1.call-done = bf16[128,2048]{1,0:T(8,128)(2,1)} async-done(((bf16[512,2048]{1,0:T(8,128)(2,1)}), bf16[128,2048]{1,0:T(8,128)(2,1)}) %reduce-scatter.6.cloned.1.call-update) | async-done | bytes 524304 | tf_op jit(solution)/shard_map/reduce_scatter | solution.py:104
  468.7 1.3 add_convert_fusion.1
  470.0 8.6 %collective-permute-done.3 = bf16[128,2048]{1,0:T(8,128)(2,1)S(1)} collective-permute-done((bf16[128,2048]{1,0:T(8,128)(2,1)S(1)}, bf16[128,2048]{1,0:T(8,128)(2,1)S(1)}, u32[]{:S(2)}, u32[]{:S(2)}) %collective-permute-start.3) | collective-permute-done | bytes 524320 | tf_op jit(solution)/shard_map/ppermute | solution.py:22
  478.6 8.6 %collective-permute-done.4 = bf16[128,2048]{1,0:T(8,128)(2,1)S(1)} collective-permute-done((bf16[128,2048]{1,0:T(8,128)(2,1)S(1)}, bf16[128,2048]{1,0:T(8,128)(2,1)S(1)}, u32[]{:S(2)}, u32[]{:S(2)}) %collective-permute-start.4) | collective-permute-done | bytes 524320 | tf_op jit(solution)/shard_map/ppermute | solution.py:22
  487.2 8.6 %collective-permute-done.5 = bf16[128,2048]{1,0:T(8,128)(2,1)S(1)} collective-permute-done((bf16[128,2048]{1,0:T(8,128)(2,1)S(1)}, bf16[128,2048]{1,0:T(8,128)(2,1)S(1)}, u32[]{:S(2)}, u32[]{:S(2)}) %collective-permute-start.5) | collective-permute-done | bytes 524320 | tf_op jit(solution)/shard_map/ppermute | solution.py:22
  495.9 3.6 fusion.6
  499.5 3.6 fusion.42
  503.2 9.7 %convolution_convert_fusion = bf16[512,2048]{1,0:T(8,128)(2,1)} fusion(bf16[896,2048]{1,0:T(8,128)(2,1)} %all-gather.12.cloned.1.call-done, f32[512,896]{1,0:T(8,128)} %fusion.42, bf16[2048,896]{1,0:T(8,128)(2,1)} %all-gather.10.cloned.1.call-done, bf16[512,2048]{1,0:T(8,128)(2,1)S(1)} %get-tuple-element.11, f32[2048]{0:T(1024)S(1)} %copy-done.10, ...), kind=kOutput, calls=%fused_computation.31 | convolution fusion | flops 3766091776 | bytes 13379584 | tf_op jit(solution)/shard_map/dot_general | solution.py:50
  512.9 31.3 %reduce-scatter.8.cloned.1.call-done = bf16[128,2048]{1,0:T(8,128)(2,1)} async-done(((bf16[512,2048]{1,0:T(8,128)(2,1)}), bf16[128,2048]{1,0:T(8,128)(2,1)}) %reduce-scatter.8.cloned.1.call-update) | async-done | bytes 524304 | tf_op jit(solution)/shard_map/reduce_scatter | solution.py:55
  544.2 2.0 add_convert_fusion
  (54 shorter events, 6.1 us)
Async XLA Ops:
  6.5 77.2 %copy-start.8 = (f32[2048]{0:T(1024)S(1)}, f32[2048]{0:T(1024)}, u32[]{:S(2)}) copy-start(f32[2048]{0:T(1024)} %param.17) | copy-start | bytes 24580
  6.5 77.2 %all-gather.8.cloned.1.call-start = ((), (), s32[]{:S(2)}) async-start(), calls=%async_computation.3 | async-start | bytes 4587520 | tf_op jit(solution)/shard_map/all_gather | solution.py:45
  7.3 148.8 %all-gather.10.cloned.1.call-start = ((), (), s32[]{:S(2)}) async-start(), calls=%async_computation.4 | async-start | bytes 4587520 | tf_op jit(solution)/shard_map/all_gather | solution.py:46
  8.0 220.3 %all-gather.12.cloned.1.call-start = ((), (), s32[]{:S(2)}) async-start(), calls=%async_computation.5 | async-start | bytes 4587520 | tf_op jit(solution)/shard_map/all_gather | solution.py:52
  8.7 259.1 %reduce-scatter.4.cloned.1.call-start = ((), (), s32[]{:S(2)}) async-start(), calls=%async_computation.6 | async-start | bytes 2621440 | tf_op jit(solution)/shard_map/reduce_scatter | solution.py:55
  8.8 9.5 %collective-permute-start = (bf16[128,2048]{1,0:T(8,128)(2,1)}, bf16[128,2048]{1,0:T(8,128)(2,1)S(1)}, u32[]{:S(2)}, u32[]{:S(2)}) collective-permute-start(bf16[128,2048]{1,0:T(8,128)(2,1)} %param.16), channel_id=1, source_target_pairs={{0,1},{1,2},{2,3},{3,0},{4,5},{5,6},{6,7},{7,4},{8,9},{9,10},{10,1... | collective-permute-start | bytes 1572872 | tf_op jit(solution)/shard_map/ppermute | solution.py:22
  18.3 8.6 %collective-permute-start.1 = (bf16[128,2048]{1,0:T(8,128)(2,1)S(1)}, bf16[128,2048]{1,0:T(8,128)(2,1)S(1)}, u32[]{:S(2)}, u32[]{:S(2)}) collective-permute-start(bf16[128,2048]{1,0:T(8,128)(2,1)S(1)} %collective-permute-done), channel_id=1, source_target_pairs={{0,1},{1,2},{2,3},{3,0},{4,5},{5,6},{6,7},{7,4},{8,9},{9,10},{10,1... | collective-permute-start | bytes 1572872 | tf_op jit(solution)/shard_map/ppermute | solution.py:22
  26.9 8.7 %collective-permute-start.2 = (bf16[128,2048]{1,0:T(8,128)(2,1)S(1)}, bf16[128,2048]{1,0:T(8,128)(2,1)}, u32[]{:S(2)}, u32[]{:S(2)}) collective-permute-start(bf16[128,2048]{1,0:T(8,128)(2,1)S(1)} %collective-permute-done.1), channel_id=1, source_target_pairs={{0,1},{1,2},{2,3},{3,0},{4,5},{5,6},{6,7},{7,4},{8,9},{9,10},{10,1... | collective-permute-start | bytes 1572872 | tf_op jit(solution)/shard_map/ppermute | solution.py:22
  89.4 178.5 %copy-start.2 = (bf16[128,2048]{1,0:T(8,128)(2,1)S(1)}, bf16[128,2048]{1,0:T(8,128)(2,1)}, u32[]{:S(2)}) copy-start(bf16[128,2048]{1,0:T(8,128)(2,1)} %param.16) | copy-start | bytes 1572868
  238.0 101.8 %copy-start.9 = (f32[2048]{0:T(1024)S(1)}, f32[2048]{0:T(1024)}, u32[]{:S(2)}) copy-start(f32[2048]{0:T(1024)} %param.22) | copy-start | bytes 24580
  238.0 54.6 %all-gather.14.cloned.1.call-start = ((), (), s32[]{:S(2)}) async-start(), calls=%async_computation.7 | async-start | bytes 2621440 | tf_op jit(solution)/shard_map/all_gather | solution.py:72
  269.9 69.8 %all-gather.18.cloned.1.call-start = ((), (), s32[]{:S(2)}) async-start(), calls=%async_computation.9 | async-start | bytes 2621440 | tf_op jit(solution)/shard_map/all_gather | solution.py:79
  270.5 115.3 %all-gather.16.cloned.1.call-start = ((), (), s32[]{:S(2)}) async-start(), calls=%async_computation.8 | async-start | bytes 2621440 | tf_op jit(solution)/shard_map/all_gather | solution.py:78
  271.2 160.6 %all-gather.20.cloned.1.call-start = ((), (), s32[]{:S(2)}) async-start(), calls=%async_computation.10 | async-start | bytes 2621440 | tf_op jit(solution)/shard_map/all_gather | solution.py:101
  272.0 196.7 %reduce-scatter.6.cloned.1.call-start = ((), (), s32[]{:S(2)}) async-start(), calls=%async_computation.11 | async-start | bytes 2621440 | tf_op jit(solution)/shard_map/reduce_scatter | solution.py:104
  294.7 56.5 %copy-start.4 = (f32[512]{0:T(512)S(1)}, f32[512]{0:T(512)}, u32[]{:S(2)}) copy-start(f32[512]{0:T(512)} %param.26) | copy-start | bytes 6148
  294.7 56.5 %copy-start.5 = (f32[512]{0:T(512)S(1)}, f32[512]{0:T(512)}, u32[]{:S(2)}) copy-start(f32[512]{0:T(512)} %param.25) | copy-start | bytes 6148
  294.7 58.8 %copy-start.3 = (bf16[4,128,128]{2,1,0:T(8,128)(2,1)S(1)}, bf16[4,128,128]{2,1,0:T(8,128)(2,1)}, u32[]{:S(2)}) copy-start(bf16[4,128,128]{2,1,0:T(8,128)(2,1)} %param.27) | copy-start | bytes 393220
  294.7 58.8 %copy-start.6 = (f32[4,128]{1,0:T(4,128)S(1)}, f32[4,128]{1,0:T(4,128)}, u32[]{:S(2)}) copy-start(f32[4,128]{1,0:T(4,128)} %param.28) | copy-start | bytes 6148
  344.5 87.4 %copy-start.1 = (bf16[512,2048]{1,0:T(8,128)(2,1)S(1)}, bf16[512,2048]{1,0:T(8,128)(2,1)}, u32[]{:S(2)}) copy-start(bf16[512,2048]{1,0:T(8,128)(2,1)} %all-gather.14.cloned.1.call-done) | copy-start | bytes 6291460
  431.9 36.8 %copy-start = (bf16[128,2048]{1,0:T(8,128)(2,1)S(1)}, bf16[128,2048]{1,0:T(8,128)(2,1)}, u32[]{:S(2)}) copy-start(bf16[128,2048]{1,0:T(8,128)(2,1)} %add_convert_fusion.3) | copy-start | bytes 1572868
  438.5 61.0 %copy-start.10 = (f32[2048]{0:T(1024)S(1)}, f32[2048]{0:T(1024)}, u32[]{:S(2)}) copy-start(f32[2048]{0:T(1024)} %param.18) | copy-start | bytes 24580
  438.5 105.7 %reduce-scatter.8.cloned.1.call-start = ((), (), s32[]{:S(2)}) async-start(), calls=%async_computation.12 | async-start | bytes 2621440 | tf_op jit(solution)/shard_map/reduce_scatter | solution.py:55
  468.7 30.9 %copy-start.7 = (bf16[2048,896]{1,0:T(8,128)(2,1)S(1)}, bf16[2048,896]{1,0:T(8,128)(2,1)}, u32[]{:S(2)}) copy-start(bf16[2048,896]{1,0:T(8,128)(2,1)} %all-gather.8.cloned.1.call-done) | copy-start | bytes 11010052
  470.0 8.7 %collective-permute-start.3 = (bf16[128,2048]{1,0:T(8,128)(2,1)S(1)}, bf16[128,2048]{1,0:T(8,128)(2,1)S(1)}, u32[]{:S(2)}, u32[]{:S(2)}) collective-permute-start(bf16[128,2048]{1,0:T(8,128)(2,1)S(1)} %add_convert_fusion.1), channel_id=1, source_target_pairs={{0,1},{1,2},{2,3},{3,0},{4,5},{5,6},{6,7},{7,4},{8,9},{9,10},{10,1... | collective-permute-start | bytes 1572872 | tf_op jit(solution)/shard_map/ppermute | solution.py:22
  478.6 8.6 %collective-permute-start.4 = (bf16[128,2048]{1,0:T(8,128)(2,1)S(1)}, bf16[128,2048]{1,0:T(8,128)(2,1)S(1)}, u32[]{:S(2)}, u32[]{:S(2)}) collective-permute-start(bf16[128,2048]{1,0:T(8,128)(2,1)S(1)} %collective-permute-done.3), channel_id=1, source_target_pairs={{0,1},{1,2},{2,3},{3,0},{4,5},{5,6},{6,7},{7,4},{8,9},{9,10},{10,1... | collective-permute-start | bytes 1572872 | tf_op jit(solution)/shard_map/ppermute | solution.py:22
  487.2 8.6 %collective-permute-start.5 = (bf16[128,2048]{1,0:T(8,128)(2,1)S(1)}, bf16[128,2048]{1,0:T(8,128)(2,1)S(1)}, u32[]{:S(2)}, u32[]{:S(2)}) collective-permute-start(bf16[128,2048]{1,0:T(8,128)(2,1)S(1)} %collective-permute-done.4), channel_id=1, source_target_pairs={{0,1},{1,2},{2,3},{3,0},{4,5},{5,6},{6,7},{7,4},{8,9},{9,10},{10,1... | collective-permute-start | bytes 1572872 | tf_op jit(solution)/shard_map/ppermute | solution.py:22
Sparse Core Ops, SparseCore 0:
  8.9 74.8 all-gather.7
  85.3 70.6 all-gather.9
  157.6 70.6 all-gather.11
  238.1 29.7 reduce-scatter.3
  270.0 22.5 all-gather.13
  294.0 45.6 all-gather.17
  341.3 44.4 all-gather.15
  387.4 44.4 all-gather.19
  438.6 29.9 reduce-scatter.5
  513.0 31.1 reduce-scatter.7
